TPU v7x, 32 devices: a whole 2x2x4 slice. The times are simulated.
32 devices in a mesh: grp: 2 (over y), sp: 4 (over z), tp: 4 (over x, core).
Axes of the slice: x: 2, y: 2, z: 4, core: 2. Of those that a mesh axis runs over, the one named last changes fastest.
Arguments:
- tokens: bfloat16 [16384, 2048], P(('grp', 'sp')), parts along dimension 0, may hold values from -6 to 6
- in_gain: float32 [2048], replicated, may hold values from 0.1 to 1.9
- w_input: bfloat16 [2048, 2048], P(None, 'tp'), may hold values from -0.125 to 0.125
- w_gate: bfloat16 [2048, 2048], P(None, 'tp'), may hold values from -4 to 4
- conv_taps: float32 [4, 2048], P(None, 'tp'), may hold values from -3 to 3
- w_rate: bfloat16 [8, 256, 256], P('tp'), may hold values from -0.375 to 0.375
- w_inlet: bfloat16 [8, 256, 256], P('tp'), may hold values from -0.375 to 0.375
- decay_param: float32 [2048], P('tp'), may hold values from 3 to 25
- decay_bias: float32 [8, 16384], P('tp', ('grp', 'sp')), parts along dimension 1, may hold values from -1.5 to 0
- out_gain: float32 [2048], P('tp'), may hold values from 0.1 to 1.9
- w_out: bfloat16 [2048, 2048], P('sp'), may hold values from -0.125 to 0.125
Outputs:
- mixer_out: bfloat16 [16384, 2048], P(('grp', 'sp', 'tp')), parts along dimension 0
There are 2 independent parts, one for each index of `grp`. A program takes and returns all parts, laid end to end along the dimension named above; an argument that names none is the same for every part. Nothing has to cross between parts.
All inputs are finite; a program needn't handle non-finite values.
Results may differ from a plain program's by a relative error of at most 0.013.
Values may be sent and summed in bfloat16 or wider, within the bound.
A program may use at most 128 MiB of HBM per device.

v0:
```python
import jax
import jax.numpy as jnp
from jax import lax
from jax.sharding import PartitionSpec as P


def from_behind(array, axis, by):
    peers = lax.axis_size(axis)
    pairs = [(i, i + by) for i in range(peers) if 0 <= i + by < peers]
    return lax.ppermute(array, axis, pairs)


def prefix(array, axis, combine, identity):
    peers, position = (lax.axis_size(axis), lax.axis_index(axis))
    everything = jax.tree.map(lambda part: lax.all_gather(part, axis), array)
    start = jax.tree.map(
        lambda part, zero: jnp.broadcast_to(jnp.asarray(zero, part.dtype), part.shape),
        array,
        identity,
    )

    def hop(k, before):
        reached = k < position
        new = combine(before, jax.tree.map(lambda part: part[k], everything))
        return jax.tree.map(lambda a, b: jnp.where(reached, a, b), new, before)

    return lax.fori_loop(0, peers, hop, start)


def combine_pairs(first_pair, second_pair):
    return (first_pair[0] * second_pair[0], second_pair[0] * first_pair[1] + second_pair[1])


def blocked_scan(decay_factor, drive_term):
    row_count, width = decay_factor.shape
    block_count = row_count // 8
    decay_blocks = decay_factor.reshape(block_count, 8, width)
    drive_blocks = drive_term.reshape(block_count, 8, width)
    running_prod = decay_blocks[:, 0]
    running_state = drive_blocks[:, 0]
    prod_list = [running_prod]
    state_list = [running_state]
    for inner in range(1, 8):
        factor = decay_blocks[:, inner]
        running_prod = factor * running_prod
        running_state = factor * running_state + drive_blocks[:, inner]
        prod_list.append(running_prod)
        state_list.append(running_state)
    prod_inner = jnp.stack(prod_list, axis=1)
    state_inner = jnp.stack(state_list, axis=1)
    total_prod = running_prod
    total_state = running_state
    stride = 1
    while stride < block_count:
        earlier_prod = jnp.concatenate(
            [jnp.ones((stride, width), jnp.float32), total_prod[: block_count - stride]], axis=0
        )
        earlier_state = jnp.concatenate(
            [jnp.zeros((stride, width), jnp.float32), total_state[: block_count - stride]], axis=0
        )
        total_prod, total_state = combine_pairs(
            (earlier_prod, earlier_state), (total_prod, total_state)
        )
        stride = stride * 2
    before_prod = jnp.concatenate(
        [jnp.ones((1, width), jnp.float32), total_prod[: block_count - 1]], axis=0
    )
    before_state = jnp.concatenate(
        [jnp.zeros((1, width), jnp.float32), total_state[: block_count - 1]], axis=0
    )
    full_prod = prod_inner * before_prod[:, None, :]
    full_local = state_inner + prod_inner * before_state[:, None, :]
    return (full_prod.reshape(row_count, width), full_local.reshape(row_count, width))


def body(
    tokens,
    in_gain,
    w_input,
    w_gate,
    conv_taps,
    w_rate,
    w_inlet,
    decay_param,
    decay_bias,
    out_gain,
    w_out,
):
    row_count = tokens.shape[0]
    channels = w_input.shape[1]
    heads_here = w_rate.shape[0]
    head_size = w_rate.shape[1]
    conv_reach = conv_taps.shape[0] - 1
    as_float = tokens.astype(jnp.float32)
    inv_norm = lax.rsqrt(jnp.mean(as_float * as_float, axis=1, keepdims=True) + 1e-06)
    normed = (as_float * inv_norm * in_gain).astype(jnp.bfloat16)
    projected = jnp.dot(normed, w_input, preferred_element_type=jnp.float32).astype(jnp.bfloat16)
    gate_raw = jnp.dot(normed, w_gate, preferred_element_type=jnp.float32).astype(jnp.bfloat16)
    prior_rows = from_behind(projected[row_count - conv_reach :], "sp", 1)
    padded = jnp.concatenate([prior_rows, projected], axis=0).astype(jnp.float32)
    summed = padded[0:row_count] * conv_taps[0]
    for offset in range(1, conv_reach + 1):
        summed = summed + padded[offset : offset + row_count] * conv_taps[offset]
    convolved = summed.astype(jnp.bfloat16)
    per_head = convolved.reshape(row_count, heads_here, head_size)
    rate_gate = jax.nn.sigmoid(
        jnp.einsum("shi,hij->shj", per_head, w_rate, preferred_element_type=jnp.float32)
    ).reshape(row_count, channels)
    input_gate = jax.nn.sigmoid(
        jnp.einsum("shi,hij->shj", per_head, w_inlet, preferred_element_type=jnp.float32)
    ).reshape(row_count, channels)
    head_bias = jnp.repeat(jnp.transpose(decay_bias), head_size, axis=1)
    log_decay = -8.0 * rate_gate * jax.nn.softplus(-decay_param) + head_bias
    decay_factor = jnp.exp(log_decay)
    drive_term = jnp.sqrt(-jnp.expm1(2.0 * log_decay)) * input_gate * convolved.astype(jnp.float32)
    half_width = channels // 2
    unit_half = (jnp.ones((half_width,), jnp.float32), jnp.zeros((half_width,), jnp.float32))
    prod_first, local_first = blocked_scan(decay_factor[:, :half_width], drive_term[:, :half_width])
    carry_first = prefix((prod_first[-1], local_first[-1]), "sp", combine_pairs, unit_half)[1]
    prod_second, local_second = blocked_scan(
        decay_factor[:, half_width:], drive_term[:, half_width:]
    )
    carry_second = prefix((prod_second[-1], local_second[-1]), "sp", combine_pairs, unit_half)[1]
    full_state = jnp.concatenate(
        [local_first + prod_first * carry_first, local_second + prod_second * carry_second], axis=1
    )
    gated_out = full_state * jax.nn.gelu(gate_raw.astype(jnp.float32))
    square_total = lax.psum(jnp.sum(gated_out * gated_out, axis=1), "tp")
    out_scale = lax.rsqrt(square_total / (channels * lax.axis_size("tp")) + 1e-06)
    normed_out = (gated_out * out_scale[:, None] * out_gain).astype(jnp.bfloat16)
    token_matrix = lax.all_to_all(normed_out, "tp", split_axis=0, concat_axis=1, tiled=True)
    projected_out = jnp.dot(
        token_matrix,
        lax.all_gather(w_out, "sp", axis=0, tiled=True),
        preferred_element_type=jnp.float32,
    )
    return projected_out.astype(jnp.bfloat16)


def solution(mesh):
    return jax.shard_map(
        body,
        mesh=mesh,
        in_specs=(
            P(("grp", "sp"), None),
            P(),
            P(None, "tp"),
            P(None, "tp"),
            P(None, "tp"),
            P("tp", None, None),
            P("tp", None, None),
            P("tp"),
            P("tp", ("grp", "sp")),
            P("tp"),
            P("sp", None),
        ),
        out_specs=P(("grp", "sp", "tp"), None),
        check_vma=False,
    )
```

profile of v0, /device:TPU:24, one launch (start us, length us, event | category | flops | bytes accessed | tf_op | source)
XLA Modules:
  0.0 219.7 jit_solution(8555406031190117634)
XLA Ops:
  6.5 5.2 %fusion = f32[2048]{0:T(1024)S(1)} fusion(bf16[2048,2048]{1,0:T(8,128)(2,1)} %param.15), kind=kLoop, calls=%fused_computation.8 | loop fusion | flops 12580864 | bytes 8396800 | tf_op jit(solution)/shard_map/reduce_sum | solution.py:95
  12.5 6.4 %convolution_convert_fusion.2 = bf16[2048,512]{1,0:T(8,128)(2,1)S(1)} fusion(bf16[2048,512]{1,0:T(8,128)(2,1)} %param.17, bf16[2048,2048]{1,0:T(8,128)(2,1)S(1)} %copy-done.6, f32[2048]{0:T(1024)S(1)} %copy-done.18, f32[2048]{0:T(1024)S(1)} %add_rsqrt_fusion.1), kind=kOutput, calls=%fused_computation.37 | convolution fusion | flops 4312793088 | bytes 12599296 | tf_op jit(solution)/shard_map/dot_general | solution.py:97
  20.3 1.8 collective-permute-start
  22.5 2.5 %broadcast_in_dim.4 = f32[2048,2,256]{2,1,0:T(2,128)S(1)} broadcast(f32[2048,2]{1,0:T(8,128)S(1)} %copy.106), dimensions={0,1} | broadcast | bytes 4210688 | tf_op jit(solution)/shard_map/broadcast_in_dim | solution.py:112
  25.0 2.4 %copy.192 = f32[256,8,2,256]{3,1,2,0:T(8,128)} copy(f32[256,8,2,256]{3,2,1,0:T(2,128)S(1)} %bitcast.123) | data formatting | bytes 8388608
  27.3 2.2 %maximum_convert_fusion = f32[2051,512]{1,0:T(8,128)S(1)} fusion(bf16[2048,512]{1,0:T(8,128)(2,1)} %copy-done.7, bf16[3,512]{1,0:T(4,128)(2,1)S(1)} %collective-permute-done), kind=kLoop, calls=%fused_computation.38 | loop fusion | flops 4200448 | bytes 6300672 | tf_op jit(solution)/shard_map/convert_element_type | solution.py:100
  29.6 1.9 fusion.10
  31.6 3.4 %add_divide_fusion.1 = f32[2,2048,256]{1,2,0:T(8,128)} fusion(bf16[2,256,256]{2,1,0:T(8,128)(2,1)S(1)} %copy-done.16, bf16[256,2,8,256]{3,2,1,0:T(8,128)(2,1)S(1)} %bitcast.140), kind=kOutput, calls=%fused_computation.34 | convolution fusion | flops 540016640 | bytes 6553600 | tf_op jit(solution)/shard_map/shi,hij->shj/dot_general | solution.py:107
  35.1 5.6 %copy.151 = f32[2048,512]{1,0:T(8,128)} copy(f32[2048,512]{0,1:T(8,128)} %bitcast.127) | data formatting | bytes 8388608 | tf_op jit(solution)/shard_map/reshape | solution.py:108
  40.7 5.0 %add_divide_fusion = f32[2,2048,256]{1,2,0:T(8,128)} fusion(bf16[2,256,256]{2,1,0:T(8,128)(2,1)S(1)} %copy-done.17, bf16[256,2,8,256]{3,2,1,0:T(8,128)(2,1)} %bitcast.141), kind=kOutput, calls=%fused_computation.32 | convolution fusion | flops 540016640 | bytes 6553600 | tf_op jit(solution)/shard_map/shi,hij->shj/dot_general | solution.py:110
  45.7 5.4 %copy.152 = f32[2048,512]{1,0:T(8,128)} copy(f32[2048,512]{0,1:T(8,128)} %bitcast.126) | data formatting | bytes 8388608 | tf_op jit(solution)/shard_map/reshape | solution.py:111
  51.1 12.7 %convert_multiply_fusion.5 = (f32[2048,512]{1,0:T(8,128)S(1)}, f32[2048,512]{1,0:T(8,128)S(1)}) fusion(f32[2048,512]{1,0:T(8,128)} %copy.152, f32[2048,512]{1,0:T(8,128)} %bitcast.124, f32[2048,512]{1,0:T(8,128)} %copy.151, f32[512]{0:T(512)S(1)} %fusion.26, f32[512]{0:T(512)S(1)} %bitcast.158, f32[2051,512]{1,0:T(8,128)} %copy-done.1, f32[512]{0:T(512)S(1)} %bitcast.160, ...), kind=kLoop, calls=%fused_computation.31 | loop fusion | flops 15728640 | bytes 37758976 | tf_op jit(solution)/shard_map/mul | solution.py:115
  72.8 9.3 %all-gather.1 = f32[4,1,256]{2,1,0:T(1,128)S(1)} all-gather(f32[1,1,256]{2,1,0:T(1,128)S(1)} %slice_bitcast_fusion.8), channel_id=1, replica_groups=mesh['grp'=2,'sp'=4,'tp'=4] {'sp'}, dimensions={0}, use_global_device_ids=true | all-gather | bytes 5120 | tf_op jit(solution)/shard_map/all_gather | solution.py:15
  83.3 20.1 %all-gather = f32[4,1,256]{2,1,0:T(1,128)S(1)} all-gather(f32[1,1,256]{2,1,0:T(1,128)S(1)} %slice_bitcast_fusion.9), channel_id=1, replica_groups=mesh['grp'=2,'sp'=4,'tp'=4] {'sp'}, dimensions={0}, use_global_device_ids=true | all-gather | bytes 5120 | tf_op jit(solution)/shard_map/all_gather | solution.py:15
  110.3 7.5 %all-gather.3 = f32[4,1,256]{2,1,0:T(1,128)S(1)} all-gather(f32[1,1,256]{2,1,0:T(1,128)S(1)} %slice_bitcast_fusion.6), channel_id=1, replica_groups=mesh['grp'=2,'sp'=4,'tp'=4] {'sp'}, dimensions={0}, use_global_device_ids=true | all-gather | bytes 5120 | tf_op jit(solution)/shard_map/all_gather | solution.py:15
  119.1 18.3 %all-gather.2 = f32[4,1,256]{2,1,0:T(1,128)S(1)} all-gather(f32[1,1,256]{2,1,0:T(1,128)S(1)} %slice_bitcast_fusion.7), channel_id=1, replica_groups=mesh['grp'=2,'sp'=4,'tp'=4] {'sp'}, dimensions={0}, use_global_device_ids=true | all-gather | bytes 5120 | tf_op jit(solution)/shard_map/all_gather | solution.py:15
  137.6 5.9 %multiply_add_fusion.3 = f32[2048,256]{1,0:T(8,128)} fusion(f32[256]{0:T(256)S(1)} %get-tuple-element.193, f32[256,8,256]{2,0,1:T(8,128)} %copy-done.2, f32[256,8,256]{2,0,1:T(8,128)} %copy-done.3), kind=kLoop, calls=%fused_computation.51 | loop fusion | flops 1048576 | bytes 6292480 | tf_op jit(solution)/shard_map/add | solution.py:125
  143.7 4.7 %multiply_add_fusion.1 = f32[2048,256]{1,0:T(8,128)S(1)} fusion(f32[256]{0:T(256)S(1)} %get-tuple-element.194, f32[256,8,256]{2,0,1:T(8,128)} %copy-done.4, f32[256,8,256]{2,0,1:T(8,128)} %copy-done.5), kind=kLoop, calls=%fused_computation.49 | loop fusion | flops 1048576 | bytes 6292480 | tf_op jit(solution)/shard_map/add | solution.py:125
  148.4 9.6 %multiply_reduce_fusion = (f32[2048]{0:T(1024)S(1)}, f32[2048,512]{1,0:T(8,128)}) fusion(bf16[2048,512]{1,0:T(8,128)(2,1)S(1)} %copy-done, bf16[2048,2048]{1,0:T(8,128)(2,1)} %param.15, f32[2048]{0:T(1024)S(1)} %copy-done.18, f32[2048]{0:T(1024)S(1)} %add_rsqrt_fusion.1, f32[2048,256]{1,0:T(8,128)S(1)} %multiply_add_fusion.1, f32[2048,256]{1,0:T(8,128)S(1)} %copy-done.9), kind=kOutput, calls=%fused_computation.30 | convolution fusion | flops 4326422528 | bytes 18898944 | tf_op jit(solution)/shard_map/dot_general | solution.py:98
  158.0 6.1 %psum.7 = f32[2048]{0:T(1024)S(1)} all-reduce(f32[2048]{0:T(1024)S(1)} %get-tuple-element.355), channel_id=1, replica_groups=mesh['grp'=2,'sp'=4,'tp'=4] {'tp'}, use_global_device_ids=true, to_apply=%region_6.7 | all-reduce | flops 2048 | bytes 16384 | tf_op jit(solution)/shard_map/psum | solution.py:128
  164.1 3.9 %multiply_convert_fusion = bf16[2048,512]{1,0:T(8,128)(2,1)} fusion(f32[2048,512]{1,0:T(8,128)} %get-tuple-element.356, f32[512]{0:T(512)S(1)} %copy-done.14, f32[2048]{0:T(1024)S(1)} %add_rsqrt_fusion), kind=kLoop, calls=%fused_computation.29 | loop fusion | flops 3145728 | bytes 6301696 | tf_op jit(solution)/shard_map/convert_element_type | solution.py:130
  168.1 4.2 %copy.148 = bf16[4,512,512]{1,2,0:T(8,128)(2,1)} copy(bf16[4,512,512]{2,1,0:T(8,128)(2,1)} %bitcast.125) | data formatting | bytes 4194304 | tf_op jit(solution)/shard_map/all_to_all | solution.py:131
  172.3 30.4 %all_to_all.19 = bf16[4,512,512]{1,2,0:T(8,128)(2,1)} all-to-all(bf16[4,512,512]{1,2,0:T(8,128)(2,1)} %copy.148), channel_id=1, replica_groups=mesh['grp'=2,'sp'=4,'tp'=4] {'tp'}, dimensions={0} | all-to-all | bytes 4194304 | tf_op jit(solution)/shard_map/all_to_all | solution.py:131
  202.6 9.9 %convolution_convert_fusion = bf16[512,2048]{1,0:T(8,128)(2,1)} fusion(bf16[512,2048]{0,1:T(8,128)(2,1)} %bitcast.142, bf16[2048,2048]{1,0:T(8,128)(2,1)} %all-gather.6.cloned.1.call-done), kind=kOutput, calls=%fused_computation.35 | convolution fusion | flops 4296015872 | bytes 12582912 | tf_op jit(solution)/shard_map/dot_general | solution.py:132
  (164 shorter events, 20.9 us)
Async XLA Ops:
  6.5 141.8 %copy-start = (bf16[2048,512]{1,0:T(8,128)(2,1)S(1)}, bf16[2048,512]{1,0:T(8,128)(2,1)}, u32[]{:S(2)}) copy-start(bf16[2048,512]{1,0:T(8,128)(2,1)} %param.18) | copy-start | bytes 6291460
  6.5 5.3 %copy-start.18 = (f32[2048]{0:T(1024)S(1)}, f32[2048]{0:T(1024)}, u32[]{:S(2)}) copy-start(f32[2048]{0:T(1024)} %param.16) | copy-start | bytes 24580
  6.5 196.1 %all-gather.6.cloned.1.call-start = ((), (), s32[]{:S(2)}) async-start(), calls=%async_computation.1 | async-start | bytes 10485760 | tf_op jit(solution)/shard_map/all_gather | solution.py:134
  6.5 5.9 %copy-start.6 = (bf16[2048,2048]{1,0:T(8,128)(2,1)S(1)}, bf16[2048,2048]{1,0:T(8,128)(2,1)}, u32[]{:S(2)}) copy-start(bf16[2048,2048]{1,0:T(8,128)(2,1)} %param.15) | copy-start | bytes 25165828
  18.9 1.3 copy-start.7
  20.2 1.8 copy-start.13
  20.2 1.8 copy-start.15
  20.3 1.9 copy-start.12
  20.3 7.1 %collective-permute-start = (bf16[3,512]{1,0:T(4,128)(2,1)S(1)}, bf16[3,512]{1,0:T(4,128)(2,1)S(1)}, u32[]{:S(2)}, u32[]{:S(2)}) collective-permute-start(bf16[3,512]{1,0:T(4,128)(2,1)S(1)} %slice.344), channel_id=1, source_target_pairs={{0,4},{4,8},{8,12},{1,5},{5,9},{9,13},{2,6},{6,10},{10,14},{3,7},{... | collective-permute-start | bytes 9224 | tf_op jit(solution)/shard_map/ppermute | solution.py:10
  29.6 2.1 copy-start.1
  29.6 2.1 copy-start.16
  31.6 3.4 %copy-start.8 = (bf16[2048,512]{1,0:T(8,128)(2,1)}, bf16[2048,512]{1,0:T(8,128)(2,1)S(1)}, u32[]{:S(2)}) copy-start(bf16[2048,512]{1,0:T(8,128)(2,1)S(1)} %fusion.10) | copy-start | bytes 6291460
  35.1 5.6 %copy-start.17 = (bf16[2,256,256]{2,1,0:T(8,128)(2,1)S(1)}, bf16[2,256,256]{2,1,0:T(8,128)(2,1)}, u32[]{:S(2)}) copy-start(bf16[2,256,256]{2,1,0:T(8,128)(2,1)} %param.21) | copy-start | bytes 786436
  69.2 0.7 copy-start.10
  69.9 0.9 copy-start.11
  69.9 1.0 slice-start
  71.4 1.3 copy-start.2
  71.4 10.6 %copy-start.3 = (f32[256,8,256]{2,0,1:T(8,128)}, f32[256,8,256]{2,0,1:T(8,128)S(1)}, u32[]{:S(2)}) copy-start(f32[256,8,256]{2,0,1:T(8,128)S(1)} %get-tuple-element.302) | copy-start | bytes 6291460
  109.0 1.3 copy-start.4
  109.0 8.8 %copy-start.5 = (f32[256,8,256]{2,0,1:T(8,128)}, f32[256,8,256]{2,0,1:T(8,128)S(1)}, u32[]{:S(2)}) copy-start(f32[256,8,256]{2,0,1:T(8,128)S(1)} %get-tuple-element.319) | copy-start | bytes 6291460
  143.7 4.7 %copy-start.9 = (f32[2048,256]{1,0:T(8,128)S(1)}, f32[2048,256]{1,0:T(8,128)}, u32[]{:S(2)}) copy-start(f32[2048,256]{1,0:T(8,128)} %multiply_add_fusion.3) | copy-start | bytes 6291460
  148.4 15.8 %copy-start.14 = (f32[512]{0:T(512)S(1)}, f32[512]{0:T(512)}, u32[]{:S(2)}) copy-start(f32[512]{0:T(512)} %param.24) | copy-start | bytes 6148
Sparse Core Ops, SparseCore 0:
  22.2 148.9 all-gather.5
where the time goes:
time: 223 us; the launch traced here: 220 us
  blocking collectives  91.7 us (41%)
  other arithmetic  40.9 us (18%)
  local copies, waits for them, and re-layouts  36.1 us (16%)
  matrix products  34.4 us (15%)
  between operations  14.5 us (7%)
    all_gather x4, blocking collectives, prefix(): everything = jax.tree.map(lambda part: lax.all_gather(part, axis), array)  55.2 us
    all_to_all x1, blocking collectives, body(): lax.all_to_all(normed_out, 'tp', split_axis=0, concat_axis=1, tiled=True)  30.4 us
    mul x1, other arithmetic, body(): jnp.sqrt(-jnp.expm1(2.0 * log_decay)) * input_gate  12.7 us
    dot_general x1, matrix products, body(): jnp.dot(token_matrix, lax.all_gather(w_out, 'sp', axis=0, tiled=True), pr...  9.9 us
    dot_general x1, matrix products, body(): jnp.dot(normed, w_gate, preferred_element_type=jnp.float32)  9.59 us
    dot_general x1, matrix products, body(): jnp.dot(normed, w_input, preferred_element_type=jnp.float32)  6.44 us
    unnamed x61, local copies, waits for them, and re-layouts  6.21 us
    psum x1, blocking collectives, body(): square_total = lax.psum(jnp.sum(gated_out * gated_out, axis=1), 'tp')  6.13 us
  transfers between devices with their start and end apart: 2, of which 0 were waited for; matrix products, arithmetic and copies ran while one was open for 39% of the time, Pallas kernels for 0%

commit v1 on v0

v1 whole, which is shorter than its diff:
```python
import functools
import jax
import jax.numpy as jnp
from jax import lax
from jax.experimental import pallas as pl
from jax.experimental.pallas import tpu as pltpu
from jax.sharding import PartitionSpec as P

MESH = pl.DeviceIdType.MESH
F32 = jnp.float32
BF16 = jnp.bfloat16
CHUNK = 256
SUB = 32


def normalize(raw, gain):
    as_float = raw.astype(F32)
    inv = lax.rsqrt(jnp.mean(as_float * as_float, axis=1, keepdims=True) + 1e-06)
    return (as_float * inv * gain).astype(BF16)


def one_minus_square(log_decay, decay):
    y = 2.0 * log_decay
    series = -y * (1.0 + y * (0.5 + y * (1.0 / 6 + y * (1.0 / 24 + y * (1.0 / 120)))))
    return jnp.where(y > -0.1, series, 1.0 - decay * decay)


def kernel(
    sizes,
    tokens, in_gain, w_input, w_gate, taps, w_rate, w_inlet, rate_scale, bias, out_gain, w_out,
    out,
    x, wi, wg, w_all, state, prod, gate, gated, arrived, total, result, halo, padded, conv,
    rate_in, inlet_in, squares, squares_in, ends, ends_in,
    x_sem, load_sem, halo_send, halo_recv, z_send, z_recv, y_send, y_recv, c_send, c_recv,
    end_send, end_recv, a_send, a_recv, q_send, q_recv, own_sem, out_sem,
):
    n_grp, n_sp, n_tp = sizes
    grp, sp, tp = lax.axis_index("grp"), lax.axis_index("sp"), lax.axis_index("tp")
    rows, width = tokens.shape
    heads, head = w_rate.shape[0], w_rate.shape[1]
    reach = taps.shape[0] - 1
    chunks = rows // CHUNK
    out_rows = rows // n_tp
    shard = w_out.shape[0]
    parts = n_grp * 2
    piece = shard // parts
    core = lax.rem(tp, 2)
    mate = tp + 1 - 2 * core
    across = 1 - grp
    quarter = grp * 2 + core
    quarter_across = across * 2 + core

    def x_copy(i):
        at = pl.ds(pl.multiple_of(i * CHUNK, CHUNK), CHUNK)
        return pltpu.make_async_copy(tokens.at[at], x.at[at], x_sem.at[i])

    loads = [
        pltpu.make_async_copy(w_input, wi, load_sem.at[0]),
        pltpu.make_async_copy(w_gate, wg, load_sem.at[1]),
        pltpu.make_async_copy(
            w_out, w_all.at[pl.ds(pl.multiple_of(sp * shard, shard), shard)], load_sem.at[2]
        ),
    ]
    loads[0].start()
    x_copy(0).start()
    loads[1].start()
    for i in range(1, chunks):
        x_copy(i).start()
    loads[2].start()

    barrier = pltpu.get_barrier_semaphore()
    for d in range(1, n_sp):
        pl.semaphore_signal(
            barrier, inc=1, device_id={"sp": lax.rem(sp + d, n_sp)}, device_id_type=MESH
        )
    for k in range(1, n_tp):
        pl.semaphore_signal(
            barrier, inc=1, device_id={"tp": lax.rem(tp + k, n_tp)}, device_id_type=MESH
        )
    pl.semaphore_signal(barrier, inc=1, device_id={"grp": across}, device_id_type=MESH)
    pl.semaphore_wait(barrier, n_sp - 1 + n_tp - 1 + 1)

    def remote(src, dst, send, recv, where):
        return pltpu.make_async_remote_copy(
            src_ref=src, dst_ref=dst, send_sem=send, recv_sem=recv,
            device_id=where, device_id_type=MESH,
        )

    halo_rows = halo.shape[0]
    halo_copy = remote(
        tokens.at[pl.ds(rows - halo_rows, halo_rows)], halo, halo_send, halo_recv,
        {"sp": lax.rem(sp + 1, n_sp)},
    )
    halo_copy.start()

    def w_rows(source, part):
        return w_all.at[pl.ds(pl.multiple_of(source * shard + part * piece, piece), piece)]

    def z_copy(d):
        return remote(
            w_out.at[pl.ds(pl.multiple_of(quarter * piece, piece), piece)],
            w_rows(sp, quarter), z_send.at[d], z_recv.at[d], {"sp": lax.rem(sp + d, n_sp)},
        )

    def y_copy(d):
        at = w_rows(lax.rem(sp + n_sp - d, n_sp), quarter)
        return remote(at, at, y_send.at[d], y_recv.at[d], {"grp": across})

    def c_copy(d, second):
        at = w_rows(
            lax.rem(sp + n_sp - d, n_sp), quarter_across if second else quarter
        )
        k = 2 * d + second
        return remote(at, at, c_send.at[k], c_recv.at[k], {"tp": mate})

    near = sorted({1, n_sp - 1})
    far = [d for d in range(2, n_sp - 1)]

    def forward_first(group):
        for d in group:
            z_copy(d).wait_recv()
            y_copy(d).start()
            c_copy(d, 0).start()

    def forward_second(group):
        for d in group:
            y_copy(d).wait_recv()
            c_copy(d, 1).start()

    for d in near:
        z_copy(d).start()

    gain_row = in_gain[...]
    sublane = lax.broadcasted_iota(jnp.int32, (SUB // 8, 8, head), 1)

    def lanes_of(h):
        return slice(h * head, (h + 1) * head)

    def spread(row):
        return jnp.broadcast_to(row, (8, row.shape[1]))

    def start_conv(h):
        before = normalize(halo[...], gain_row)
        before = jnp.dot(before, wi[:, lanes_of(h)], preferred_element_type=F32)
        before = before.astype(BF16).astype(F32)
        padded[0:8, :] = jnp.where(sp > 0, before[halo_rows - 8 :], 0.0)

    def phase_a(h, i, carry):
        lanes = lanes_of(h)
        at = pl.ds(pl.multiple_of(i * CHUNK, CHUNK), CHUNK)
        if h == 0:
            x_copy(i).wait()
            x[at, :] = normalize(x[at, :], gain_row)
        normed = x[at, :]
        projected = jnp.dot(normed, wi[:, lanes], preferred_element_type=F32)
        padded[8:, :] = projected.astype(BF16).astype(F32)
        for r in range(0, CHUNK, SUB):
            summed = padded[8 - reach + r : 8 - reach + r + SUB, :] * taps[0:1, lanes]
            for k in range(1, reach + 1):
                first = 8 - reach + k + r
                summed = summed + padded[first : first + SUB, :] * taps[k : k + 1, lanes]
            conv[r : r + SUB, :] = summed.astype(BF16)
        padded[0:8, :] = padded[CHUNK:, :]
        rate_in[...] = jnp.dot(conv[...], w_rate[h], preferred_element_type=F32)
        inlet_in[...] = jnp.dot(conv[...], w_inlet[h], preferred_element_type=F32)
        gate_raw = jnp.dot(normed, wg[:, lanes], preferred_element_type=F32)
        gate[at, lanes] = gate_raw
        bias_row = bias[h : h + 1, at]
        bias_cols = jnp.broadcast_to(bias_row, (128, CHUNK)).T
        scale = rate_scale[0:1, lanes]
        s, p = carry
        for r in range(0, CHUNK, SUB):
            here = slice(r, r + SUB)
            into = pl.ds(pl.multiple_of(i * CHUNK + r, SUB), SUB)
            raw = gate[into, lanes].astype(BF16).astype(F32)
            gate[into, lanes] = jax.nn.gelu(raw)
            bias_here = jnp.concatenate([bias_cols[here]] * (head // 128), axis=1)
            log_decay = jax.nn.sigmoid(rate_in[here, :]) * scale + bias_here
            decay = jnp.exp(log_decay)
            drive = (
                jnp.sqrt(one_minus_square(log_decay, decay))
                * jax.nn.sigmoid(inlet_in[here, :])
                * conv[here, :].astype(F32)
            )
            pt = decay.reshape(SUB // 8, 8, head)
            st = drive.reshape(SUB // 8, 8, head)
            for d in (1, 2, 4):
                inside = sublane >= d
                st = st + pt * jnp.where(inside, pltpu.roll(st, d, 1), 0.0)
                pt = pt * jnp.where(inside, pltpu.roll(pt, d, 1), 1.0)
            s_parts, p_parts = [], []
            for t in range(SUB // 8):
                s_parts.append(st[t] + pt[t] * s)
                p_parts.append(pt[t] * p)
                p_last = spread(pt[t, 7:8])
                s = spread(st[t, 7:8]) + p_last * s
                p = p_last * p
            state[into, lanes] = jnp.concatenate(s_parts, axis=0)
            prod[into, lanes] = jnp.concatenate(p_parts, axis=0)
        return s, p

    def start_carry():
        return jnp.zeros((8, head), F32), jnp.ones((8, head), F32)

    def end_copy(h, d):
        k = h * n_sp + d
        return remote(
            ends.at[h], ends_in.at[k], end_send.at[k], end_recv.at[k],
            {"sp": lax.rem(sp + d, n_sp)},
        )

    def send_ends(h, carry):
        s, p = carry
        ends[h, 0:8, :] = s
        ends[h, 8:16, :] = p
        for d in range(1, n_sp):
            end_copy(h, d).start()

    def take_ends(h):
        carry = jnp.zeros((8, head), F32)
        for d in range(n_sp - 1, 0, -1):
            end_copy(h, d).wait_recv()
            k = h * n_sp + d
            new = ends_in[k, 0:8, :] + ends_in[k, 8:16, :] * carry
            carry = jnp.where(d <= sp, new, carry)
        return carry[0:1]

    def a_copy(h, k):
        to = lax.rem(tp + k, n_tp)
        at = pl.ds(pl.multiple_of(to * out_rows, out_rows), out_rows)
        slot = h * n_tp + k
        return remote(
            gated.at[h, at], arrived.at[tp * heads + h], a_send.at[slot], a_recv.at[slot],
            {"tp": to},
        )

    def q_copy(h, k):
        to = lax.rem(tp + k, n_tp)
        slot = h * n_tp + k
        return remote(
            squares.at[h * n_tp + to], squares_in.at[tp * heads + h],
            q_send.at[slot], q_recv.at[slot], {"tp": to},
        )

    def own_copies(h):
        at = pl.ds(pl.multiple_of(tp * out_rows, out_rows), out_rows)
        return (
            pltpu.make_async_copy(gated.at[h, at], arrived.at[tp * heads + h], own_sem.at[2 * h]),
            pltpu.make_async_copy(
                squares.at[h * n_tp + tp], squares_in.at[tp * heads + h], own_sem.at[2 * h + 1]
            ),
        )

    order = list(range(2, n_tp)) + [1, 0]

    def phase_b(h, carry):
        lanes = lanes_of(h)
        for k in order:
            to = lax.rem(tp + k, n_tp)

            def block(j, _):
                sums = []
                for r in range(0, CHUNK, SUB):
                    first = j * CHUNK + r
                    at = pl.ds(pl.multiple_of(to * out_rows + first, SUB), SUB)
                    full = state[at, lanes] + prod[at, lanes] * carry
                    value = full * gate[at, lanes]
                    gated[h, at, :] = (value * out_gain[0:1, lanes]).astype(BF16)
                    square = value * value
                    part = square[:, 0:128]
                    for c in range(128, head, 128):
                        part = part + square[:, c : c + 128]
                    sums.append(part)
                row = jnp.sum(jnp.concatenate(sums, axis=0).T, axis=0, keepdims=True)
                squares[h * n_tp + to, :, pl.ds(pl.multiple_of(j * CHUNK, CHUNK), CHUNK)] = spread(row)
                return 0

            lax.fori_loop(0, out_rows // CHUNK, block, 0)
            if k == 0:
                for copy in own_copies(h):
                    copy.start()
            else:
                a_copy(h, k).start()
                q_copy(h, k).start()

    def wait_blocks(h):
        for copy in own_copies(h):
            copy.wait()
        for k in range(1, n_tp):
            a_copy(h, k).wait_recv()
            q_copy(h, k).wait_recv()

    def finish_w():
        for d in range(1, n_sp):
            c_copy(d, 0).wait_recv()
            c_copy(d, 1).wait_recv()

    tile = 512 if width % 512 == 0 else 256

    def multiply(h, columns):
        left = jnp.concatenate([arrived[k * heads + h] for k in range(n_tp)], axis=1)
        right = jnp.concatenate(
            [w_all[(k * heads + h) * head : (k * heads + h + 1) * head, columns] for k in range(n_tp)],
            axis=0,
        )
        return jnp.dot(left, right, preferred_element_type=F32)

    loads[0].wait()
    carry = start_carry()
    halo_copy.wait_recv()
    start_conv(0)
    loads[1].wait()
    carry = lax.fori_loop(0, chunks, lambda i, c: phase_a(0, i, c), carry)
    send_ends(0, carry)
    for d in far:
        z_copy(d).start()
    split = min(2, chunks)
    for h in range(1, heads):
        start_conv(h)
        carry = lax.fori_loop(0, split, functools.partial(phase_a, h), start_carry())
        phase_b(h - 1, take_ends(h - 1))
        if h == 1:
            forward_first(near)
        carry = lax.fori_loop(split, chunks, functools.partial(phase_a, h), carry)
        send_ends(h, carry)
    if heads == 1:
        forward_first(near)
    last = heads - 1
    phase_b(last, take_ends(last))
    forward_first(far)
    forward_second(near)
    forward_second(far)
    loads[2].wait()
    finish_w()
    for h in range(last):
        wait_blocks(h)

        def partial_sum(n, _, h=h):
            columns = pl.ds(pl.multiple_of(n * tile, tile), tile)
            value = multiply(h, columns)
            total[:, columns] = value if h == 0 else total[:, columns] + value
            return 0

        lax.fori_loop(0, width // tile, partial_sum, 0)
    wait_blocks(last)
    row = squares_in[0]
    for k in range(1, n_tp * heads):
        row = row + squares_in[k]
    out_scale = lax.rsqrt(row[0:1] / (n_tp * heads * head) + 1e-06)
    scale_cols = jnp.broadcast_to(out_scale, (128, out_rows)).T

    def out_copy(n):
        columns = pl.ds(pl.multiple_of(n * tile, tile), tile)
        return pltpu.make_async_copy(result.at[:, columns], out.at[:, columns], out_sem.at[n])

    def final(n, _):
        columns = pl.ds(pl.multiple_of(n * tile, tile), tile)
        value = multiply(last, columns)
        if last > 0:
            value = value + total[:, columns]
        value = value * jnp.concatenate([scale_cols] * (tile // 128), axis=1)
        result[:, columns] = value.astype(BF16)
        out_copy(n).start()
        return 0

    lax.fori_loop(0, width // tile, final, 0)

    halo_copy.wait_send()
    for d in range(1, n_sp):
        z_copy(d).wait_send()
        y_copy(d).wait_send()
        c_copy(d, 0).wait_send()
        c_copy(d, 1).wait_send()
        for h in range(heads):
            end_copy(h, d).wait_send()
    for h in range(heads):
        for k in range(1, n_tp):
            a_copy(h, k).wait_send()
            q_copy(h, k).wait_send()
    for n in range(width // tile):
        out_copy(n).wait()


def body(sizes, tokens, in_gain, w_input, w_gate, conv_taps, w_rate, w_inlet, decay_param,
         decay_bias, out_gain, w_out):
    n_grp, n_sp, n_tp = sizes
    rows, width = tokens.shape
    channels = w_input.shape[1]
    heads, head = w_rate.shape[0], w_rate.shape[1]
    out_rows = rows // n_tp
    out_width = w_out.shape[1]
    all_channels = channels * n_tp
    tile = 512 if out_width % 512 == 0 else 256
    rate_scale = (-8.0 * jax.nn.softplus(-decay_param)).reshape(1, channels)
    hbm = pl.BlockSpec(memory_space=pl.ANY)
    vmem = pl.BlockSpec(memory_space=pltpu.VMEM)
    dma = pltpu.SemaphoreType.DMA
    return pl.pallas_call(
        functools.partial(kernel, sizes),
        out_shape=jax.ShapeDtypeStruct((out_rows, out_width), BF16),
        in_specs=[hbm, vmem, hbm, hbm, vmem, vmem, vmem, vmem, vmem, vmem, hbm],
        out_specs=hbm,
        scratch_shapes=[
            pltpu.VMEM((rows, width), BF16),
            pltpu.VMEM((width, channels), BF16),
            pltpu.VMEM((width, channels), BF16),
            pltpu.VMEM((all_channels, out_width), BF16),
            pltpu.VMEM((rows, channels), F32),
            pltpu.VMEM((rows, channels), F32),
            pltpu.VMEM((rows, channels), F32),
            pltpu.VMEM((heads, rows, head), BF16),
            pltpu.VMEM((n_tp * heads, out_rows, head), BF16),
            pltpu.VMEM((out_rows, out_width), F32),
            pltpu.VMEM((out_rows, out_width), BF16),
            pltpu.VMEM((16, width), BF16),
            pltpu.VMEM((CHUNK + 8, head), F32),
            pltpu.VMEM((CHUNK, head), BF16),
            pltpu.VMEM((CHUNK, head), F32),
            pltpu.VMEM((CHUNK, head), F32),
            pltpu.VMEM((heads * n_tp, 8, out_rows), F32),
            pltpu.VMEM((n_tp * heads, 8, out_rows), F32),
            pltpu.VMEM((heads, 16, head), F32),
            pltpu.VMEM((heads * n_sp, 16, head), F32),
            dma((rows // CHUNK,)),
            dma((3,)),
            dma,
            dma,
            dma((n_sp,)),
            dma((n_sp,)),
            dma((n_sp,)),
            dma((n_sp,)),
            dma((2 * n_sp,)),
            dma((2 * n_sp,)),
            dma((heads * n_sp,)),
            dma((heads * n_sp,)),
            dma((heads * n_tp,)),
            dma((heads * n_tp,)),
            dma((heads * n_tp,)),
            dma((heads * n_tp,)),
            dma((2 * heads,)),
            dma((out_width // tile,)),
        ],
        compiler_params=pltpu.CompilerParams(
            collective_id=0, has_side_effects=True, vmem_limit_bytes=62 * 1024 * 1024
        ),
    )(
        tokens, in_gain.reshape(1, width), w_input, w_gate, conv_taps, w_rate, w_inlet,
        rate_scale, decay_bias, out_gain.reshape(1, channels), w_out,
    )


def solution(mesh):
    sizes = (mesh.shape["grp"], mesh.shape["sp"], mesh.shape["tp"])
    return jax.shard_map(
        functools.partial(body, sizes),
        mesh=mesh,
        in_specs=(
            P(("grp", "sp"), None),
            P(),
            P(None, "tp"),
            P(None, "tp"),
            P(None, "tp"),
            P("tp", None, None),
            P("tp", None, None),
            P("tp"),
            P("tp", ("grp", "sp")),
            P("tp"),
            P("sp", None),
        ),
        out_specs=P(("grp", "sp", "tp"), None),
        check_vma=False,
    )
```

time: 223 us -> 93.2 us (0.42)
  the two profiles are of different devices: /device:TPU:24 before, /device:TPU:25 now
where the time goes in v1:
time: 93.2 us; the launch traced here: 93 us
  Pallas kernels  88.6 us (95%)
  local copies, waits for them, and re-layouts  3.16 us (3%)
  other arithmetic  1.28 us (1%)
    pallas_call x1, Pallas kernels, body(): pl.pallas_call(functools.partial(kernel, sizes), out_shape=jax.ShapeDtype...  88.6 us
    unnamed x1, local copies, waits for them, and re-layouts  3.16 us

profile of v1, /device:TPU:25, one launch (start us, length us, event | category | flops | bytes accessed | tf_op | source)
XLA Modules:
  0.0 93.0 jit_solution(9410489220481305987)
XLA Ops:
  0.0 1.3 %fusion = f32[512]{0:T(512)} fusion(f32[512]{0:T(512)} %param.18), kind=kLoop, calls=%fused_computation.1 | loop fusion | flops 4096 | bytes 4096 | tf_op jit(solution)/shard_map/mul | solution.py:394
  1.3 88.6 %shard_map.109 = bf16[512,2048]{1,0:T(8,128)(2,1)} custom-call(bf16[2048,2048]{1,0:T(8,128)(2,1)} %tokens.1, f32[1,2048]{1,0:T(1,128)} %bitcast.3, bf16[2048,512]{1,0:T(8,128)(2,1)} %w_input.1, bf16[2048,512]{1,0:T(8,128)(2,1)} %w_gate.1, f32[4,512]{1,0:T(4,128)} %taps.1, bf16[2,256,256]{2,1,0:T(8,128)(2,1)} %w_rate.1, bf16[2,256,256]{2,1,0:T(8,128)(2,1)} %w_inlet.1, ...), custom_call_target="tpu_custom_call" | custom-call | tf_op jit(solution)/shard_map/pallas_call | solution.py:398
  89.9 3.2 %copy.13 = bf16[512,2048]{1,0:T(8,128)(2,1)} copy(bf16[512,2048]{1,0:T(8,128)(2,1)} %shard_map.109) | data formatting | bytes 4194304

commit v2 on v1

--- a/solution.py
+++ b/solution.py
@@ -31,7 +31,8 @@
     out,
     x, wi, wg, w_all, state, prod, gate, gated, arrived, total, result, halo, padded, conv,
     rate_in, inlet_in, squares, squares_in, ends, ends_in,
-    x_sem, load_sem, halo_send, halo_recv, z_send, z_recv, y_send, y_recv, c_send, c_recv,
+    x_sem, load_sem, halo_send, halo_recv, z_send, z_recv, x_send, x_recv, y_send, y_recv,
+    c_send, c_recv,
     end_send, end_recv, a_send, a_recv, q_send, q_recv, own_sem, out_sem,
 ):
     n_grp, n_sp, n_tp = sizes
@@ -42,13 +43,14 @@
     chunks = rows // CHUNK
     out_rows = rows // n_tp
     shard = w_out.shape[0]
-    parts = n_grp * 2
-    piece = shard // parts
+    piece = shard // (2 * n_grp * 2)
     core = lax.rem(tp, 2)
     mate = tp + 1 - 2 * core
+    side = lax.rem(tp // 2, 2)
+    beside = tp + 2 - 4 * side
     across = 1 - grp
-    quarter = grp * 2 + core
-    quarter_across = across * 2 + core
+    part = (core * n_grp + grp) * 2 + side
+    part_beside = (core * n_grp + grp) * 2 + 1 - side
 
     def x_copy(i):
         at = pl.ds(pl.multiple_of(i * CHUNK, CHUNK), CHUNK)
@@ -93,25 +95,29 @@
     )
     halo_copy.start()
 
-    def w_rows(source, part):
-        return w_all.at[pl.ds(pl.multiple_of(source * shard + part * piece, piece), piece)]
+    def w_rows(d, which, count=1):
+        source = lax.rem(sp + n_sp - d, n_sp)
+        first = pl.multiple_of(source * shard + which * piece, piece)
+        return w_all.at[pl.ds(first, count * piece)]
 
     def z_copy(d):
         return remote(
-            w_out.at[pl.ds(pl.multiple_of(quarter * piece, piece), piece)],
-            w_rows(sp, quarter), z_send.at[d], z_recv.at[d], {"sp": lax.rem(sp + d, n_sp)},
-        )
-
-    def y_copy(d):
-        at = w_rows(lax.rem(sp + n_sp - d, n_sp), quarter)
-        return remote(at, at, y_send.at[d], y_recv.at[d], {"grp": across})
-
-    def c_copy(d, second):
-        at = w_rows(
-            lax.rem(sp + n_sp - d, n_sp), quarter_across if second else quarter
-        )
+            w_out.at[pl.ds(pl.multiple_of(part * piece, piece), piece)],
+            w_rows(0, part), z_send.at[d], z_recv.at[d], {"sp": lax.rem(sp + d, n_sp)},
+        )
+
+    def x_forward(d):
+        at = w_rows(d, part)
+        return remote(at, at, x_send.at[d], x_recv.at[d], {"tp": beside})
+
+    def y_forward(d, second):
+        at = w_rows(d, part_beside if second else part)
         k = 2 * d + second
-        return remote(at, at, c_send.at[k], c_recv.at[k], {"tp": mate})
+        return remote(at, at, y_send.at[k], y_recv.at[k], {"grp": across})
+
+    def c_forward(d):
+        at = w_rows(d, core * n_grp * 2, n_grp * 2)
+        return remote(at, at, c_send.at[d], c_recv.at[d], {"tp": mate})
 
     near = sorted({1, n_sp - 1})
     far = [d for d in range(2, n_sp - 1)]
@@ -119,15 +125,32 @@
     def forward_first(group):
         for d in group:
             z_copy(d).wait_recv()
-            y_copy(d).start()
-            c_copy(d, 0).start()
+            y_forward(d, 0).start()
+            x_forward(d).start()
 
     def forward_second(group):
         for d in group:
-            y_copy(d).wait_recv()
-            c_copy(d, 1).start()
-
-    for d in near:
+            x_forward(d).wait_recv()
+            y_forward(d, 1).start()
+
+    def forward_third(group):
+        for d in group:
+            y_forward(d, 0).wait_recv()
+            y_forward(d, 1).wait_recv()
+            c_forward(d).start()
+
+    def middle():
+        forward_second(near)
+        forward_first(far)
+
+    head_last = heads - 1
+    points = {(0, chunks - 3): lambda: forward_first(near)}
+    points[(head_last, chunks - 2)] = lambda: forward_second(far)
+    if heads == 1:
+        points[(0, chunks - 2)] = middle
+        points[(0, chunks - 1)] = lambda: forward_second(far)
+
+    for d in near + far:
         z_copy(d).start()
 
     gain_row = in_gain[...]
@@ -148,6 +171,9 @@
     def phase_a(h, i, carry):
         lanes = lanes_of(h)
         at = pl.ds(pl.multiple_of(i * CHUNK, CHUNK), CHUNK)
+        for (point_head, point), action in points.items():
+            if point_head == h:
+                pl.when(i == point)(action)
         if h == 0:
             x_copy(i).wait()
             x[at, :] = normalize(x[at, :], gain_row)
@@ -292,8 +318,7 @@
 
     def finish_w():
         for d in range(1, n_sp):
-            c_copy(d, 0).wait_recv()
-            c_copy(d, 1).wait_recv()
+            c_forward(d).wait_recv()
 
     tile = 512 if width % 512 == 0 else 256
 
@@ -310,26 +335,21 @@
     halo_copy.wait_recv()
     start_conv(0)
     loads[1].wait()
-    carry = lax.fori_loop(0, chunks, lambda i, c: phase_a(0, i, c), carry)
+    carry = lax.fori_loop(0, chunks, functools.partial(phase_a, 0), carry)
     send_ends(0, carry)
-    for d in far:
-        z_copy(d).start()
     split = min(2, chunks)
     for h in range(1, heads):
         start_conv(h)
         carry = lax.fori_loop(0, split, functools.partial(phase_a, h), start_carry())
+        if h == 1:
+            middle()
         phase_b(h - 1, take_ends(h - 1))
-        if h == 1:
-            forward_first(near)
         carry = lax.fori_loop(split, chunks, functools.partial(phase_a, h), carry)
         send_ends(h, carry)
-    if heads == 1:
-        forward_first(near)
     last = heads - 1
     phase_b(last, take_ends(last))
-    forward_first(far)
-    forward_second(near)
-    forward_second(far)
+    forward_third(near)
+    forward_third(far)
     loads[2].wait()
     finish_w()
     for h in range(last):
@@ -368,9 +388,10 @@
     halo_copy.wait_send()
     for d in range(1, n_sp):
         z_copy(d).wait_send()
-        y_copy(d).wait_send()
-        c_copy(d, 0).wait_send()
-        c_copy(d, 1).wait_send()
+        x_forward(d).wait_send()
+        y_forward(d, 0).wait_send()
+        y_forward(d, 1).wait_send()
+        c_forward(d).wait_send()
         for h in range(heads):
             end_copy(h, d).wait_send()
     for h in range(heads):
@@ -431,6 +452,8 @@
             dma((n_sp,)),
             dma((2 * n_sp,)),
             dma((2 * n_sp,)),
+            dma((n_sp,)),
+            dma((n_sp,)),
             dma((heads * n_sp,)),
             dma((heads * n_sp,)),
             dma((heads * n_tp,)),

time: 93.2 us -> 73.6 us (0.79)
  the two profiles are of different devices: /device:TPU:25 before, /device:TPU:1 now
where the time goes in v2:
time: 73.6 us; the launch traced here: 73.4 us
  Pallas kernels  69 us (94%)
  local copies, waits for them, and re-layouts  3.16 us (4%)
  other arithmetic  1.28 us (2%)
    pallas_call x1, Pallas kernels, body(): pl.pallas_call(functools.partial(kernel, sizes), out_shape=jax.ShapeDtype...  69 us
    unnamed x1, local copies, waits for them, and re-layouts  3.16 us

profile of v2, /device:TPU:1, one launch (start us, length us, event | category | flops | bytes accessed | tf_op | source)
XLA Modules:
  0.0 73.4 jit_solution(1992339813401786700)
XLA Ops:
  0.0 1.3 %fusion = f32[512]{0:T(512)} fusion(f32[512]{0:T(512)} %param.18), kind=kLoop, calls=%fused_computation.1 | loop fusion | flops 4096 | bytes 4096 | tf_op jit(solution)/shard_map/mul | solution.py:415
  1.3 69.0 %shard_map.109 = bf16[512,2048]{1,0:T(8,128)(2,1)} custom-call(bf16[2048,2048]{1,0:T(8,128)(2,1)} %tokens.1, f32[1,2048]{1,0:T(1,128)} %bitcast.3, bf16[2048,512]{1,0:T(8,128)(2,1)} %w_input.1, bf16[2048,512]{1,0:T(8,128)(2,1)} %w_gate.1, f32[4,512]{1,0:T(4,128)} %taps.1, bf16[2,256,256]{2,1,0:T(8,128)(2,1)} %w_rate.1, bf16[2,256,256]{2,1,0:T(8,128)(2,1)} %w_inlet.1, ...), custom_call_target="tpu_custom_call" | custom-call | tf_op jit(solution)/shard_map/pallas_call | solution.py:419
  70.3 3.2 %copy.13 = bf16[512,2048]{1,0:T(8,128)(2,1)} copy(bf16[512,2048]{1,0:T(8,128)(2,1)} %shard_map.109) | data formatting | bytes 4194304

commit v3 on v2

--- a/solution.py
+++ b/solution.py
@@ -1,4 +1,5 @@
 import functools
+import math
 import jax
 import jax.numpy as jnp
 from jax import lax
@@ -19,10 +20,20 @@
     return (as_float * inv * gain).astype(BF16)
 
 
-def one_minus_square(log_decay, decay):
-    y = 2.0 * log_decay
-    series = -y * (1.0 + y * (0.5 + y * (1.0 / 6 + y * (1.0 / 24 + y * (1.0 / 120)))))
-    return jnp.where(y > -0.1, series, 1.0 - decay * decay)
+LN4 = 2.0 * math.log(2.0)
+GELU_A = math.sqrt(2.0 / math.pi)
+GELU_B = GELU_A * 0.044715
+
+
+def one_minus_square(log2_decay, decay):
+    a1, a2, a3, a4 = -LN4, -(LN4**2) / 2, -(LN4**3) / 6, -(LN4**4) / 24
+    series = log2_decay * (a1 + log2_decay * (a2 + log2_decay * (a3 + log2_decay * a4)))
+    return jnp.where(log2_decay > -0.025, series, 1.0 - decay * decay)
+
+
+def gelu_half(value):
+    inner = value * (GELU_A + GELU_B * (value * value))
+    return (0.25 * value) * (1.0 + jnp.tanh(inner))
 
 
 def kernel(
@@ -30,7 +41,7 @@
     tokens, in_gain, w_input, w_gate, taps, w_rate, w_inlet, rate_scale, bias, out_gain, w_out,
     out,
     x, wi, wg, w_all, state, prod, gate, gated, arrived, total, result, halo, padded, conv,
-    rate_in, inlet_in, squares, squares_in, ends, ends_in,
+    halved, rate_in, inlet_in, squares, squares_in, ends, ends_in,
     x_sem, load_sem, halo_send, halo_recv, z_send, z_recv, x_send, x_recv, y_send, y_recv,
     c_send, c_recv,
     end_send, end_recv, a_send, a_recv, q_send, q_recv, own_sem, out_sem,
@@ -165,7 +176,6 @@
     def start_conv(h):
         before = normalize(halo[...], gain_row)
         before = jnp.dot(before, wi[:, lanes_of(h)], preferred_element_type=F32)
-        before = before.astype(BF16).astype(F32)
         padded[0:8, :] = jnp.where(sp > 0, before[halo_rows - 8 :], 0.0)
 
     def phase_a(h, i, carry):
@@ -179,7 +189,7 @@
             x[at, :] = normalize(x[at, :], gain_row)
         normed = x[at, :]
         projected = jnp.dot(normed, wi[:, lanes], preferred_element_type=F32)
-        padded[8:, :] = projected.astype(BF16).astype(F32)
+        padded[8:, :] = projected
         for r in range(0, CHUNK, SUB):
             summed = padded[8 - reach + r : 8 - reach + r + SUB, :] * taps[0:1, lanes]
             for k in range(1, reach + 1):
@@ -187,26 +197,24 @@
                 summed = summed + padded[first : first + SUB, :] * taps[k : k + 1, lanes]
             conv[r : r + SUB, :] = summed.astype(BF16)
         padded[0:8, :] = padded[CHUNK:, :]
-        rate_in[...] = jnp.dot(conv[...], w_rate[h], preferred_element_type=F32)
-        inlet_in[...] = jnp.dot(conv[...], w_inlet[h], preferred_element_type=F32)
+        rate_in[...] = jnp.dot(conv[...], halved[2 * h], preferred_element_type=F32)
+        inlet_in[...] = jnp.dot(conv[...], halved[2 * h + 1], preferred_element_type=F32)
         gate_raw = jnp.dot(normed, wg[:, lanes], preferred_element_type=F32)
-        gate[at, lanes] = gate_raw
-        bias_row = bias[h : h + 1, at]
+        gate[at, lanes] = gelu_half(gate_raw)
+        bias_row = bias[h : h + 1, at] * (1.0 / math.log(2.0))
         bias_cols = jnp.broadcast_to(bias_row, (128, CHUNK)).T
         scale = rate_scale[0:1, lanes]
         s, p = carry
         for r in range(0, CHUNK, SUB):
             here = slice(r, r + SUB)
             into = pl.ds(pl.multiple_of(i * CHUNK + r, SUB), SUB)
-            raw = gate[into, lanes].astype(BF16).astype(F32)
-            gate[into, lanes] = jax.nn.gelu(raw)
             bias_here = jnp.concatenate([bias_cols[here]] * (head // 128), axis=1)
-            log_decay = jax.nn.sigmoid(rate_in[here, :]) * scale + bias_here
-            decay = jnp.exp(log_decay)
+            log2_decay = jnp.tanh(rate_in[here, :]) * scale + (bias_here + scale)
+            decay = jnp.exp2(log2_decay)
+            left = one_minus_square(log2_decay, decay)
             drive = (
-                jnp.sqrt(one_minus_square(log_decay, decay))
-                * jax.nn.sigmoid(inlet_in[here, :])
-                * conv[here, :].astype(F32)
+                left * lax.rsqrt(jnp.maximum(left, 1e-37))
+                * ((1.0 + jnp.tanh(inlet_in[here, :])) * conv[here, :].astype(F32))
             )
             pt = decay.reshape(SUB // 8, 8, head)
             st = drive.reshape(SUB // 8, 8, head)
@@ -329,6 +337,10 @@
             axis=0,
         )
         return jnp.dot(left, right, preferred_element_type=F32)
+
+    for h in range(heads):
+        halved[2 * h] = w_rate[h] * 0.5
+        halved[2 * h + 1] = w_inlet[h] * 0.5
 
     loads[0].wait()
     carry = start_carry()
@@ -412,7 +424,7 @@
     out_width = w_out.shape[1]
     all_channels = channels * n_tp
     tile = 512 if out_width % 512 == 0 else 256
-    rate_scale = (-8.0 * jax.nn.softplus(-decay_param)).reshape(1, channels)
+    rate_scale = (-4.0 / math.log(2.0) * jax.nn.softplus(-decay_param)).reshape(1, channels)
     hbm = pl.BlockSpec(memory_space=pl.ANY)
     vmem = pl.BlockSpec(memory_space=pltpu.VMEM)
     dma = pltpu.SemaphoreType.DMA
@@ -436,6 +448,7 @@
             pltpu.VMEM((16, width), BF16),
             pltpu.VMEM((CHUNK + 8, head), F32),
             pltpu.VMEM((CHUNK, head), BF16),
+            pltpu.VMEM((2 * heads, head, head), BF16),
             pltpu.VMEM((CHUNK, head), F32),
             pltpu.VMEM((CHUNK, head), F32),
             pltpu.VMEM((heads * n_tp, 8, out_rows), F32),

time: 73.6 us -> 73.1 us (level)
  no operation moved by 1% of the time
where the time goes in v3:
time: 73.1 us; the launch traced here: 72.9 us
  Pallas kernels  68.4 us (94%)
  local copies, waits for them, and re-layouts  3.16 us (4%)
  other arithmetic  1.28 us (2%)
    pallas_call x1, Pallas kernels, body(): pl.pallas_call(functools.partial(kernel, sizes), out_shape=jax.ShapeDtype...  68.4 us
    unnamed x1, local copies, waits for them, and re-layouts  3.16 us

profile of v3, /device:TPU:1, one launch (start us, length us, event | category | flops | bytes accessed | tf_op | source)
XLA Modules:
  0.0 72.9 jit_solution(7451272660544766616)
XLA Ops:
  0.0 1.3 %fusion = f32[512]{0:T(512)} fusion(f32[512]{0:T(512)} %param.18), kind=kLoop, calls=%fused_computation.1 | loop fusion | flops 4096 | bytes 4096 | tf_op jit(solution)/shard_map/mul | solution.py:427
  1.3 68.4 %shard_map.109 = bf16[512,2048]{1,0:T(8,128)(2,1)} custom-call(bf16[2048,2048]{1,0:T(8,128)(2,1)} %tokens.1, f32[1,2048]{1,0:T(1,128)} %bitcast.3, bf16[2048,512]{1,0:T(8,128)(2,1)} %w_input.1, bf16[2048,512]{1,0:T(8,128)(2,1)} %w_gate.1, f32[4,512]{1,0:T(4,128)} %taps.1, bf16[2,256,256]{2,1,0:T(8,128)(2,1)} %w_rate.1, bf16[2,256,256]{2,1,0:T(8,128)(2,1)} %w_inlet.1, ...), custom_call_target="tpu_custom_call" | custom-call | tf_op jit(solution)/shard_map/pallas_call | solution.py:431
  69.7 3.2 %copy.13 = bf16[512,2048]{1,0:T(8,128)(2,1)} copy(bf16[512,2048]{1,0:T(8,128)(2,1)} %shard_map.109) | data formatting | bytes 4194304
